TPU v7x, 32 devices: a whole 2x2x4 slice. The times are simulated.
32 devices in a mesh: ep: 4 (over y, x), tp: 8 (over z, core).
Axes of the slice: x: 2, y: 2, z: 4, core: 2. Of those that a mesh axis runs over, the one named last changes fastest.
Arguments:
- queries: bfloat16 [2, 1024, 4096], P(None, 'tp', 'ep'), may hold values from -6 to 6
- key_vectors: bfloat16 [2, 1024, 4096], P(None, 'tp', 'ep'), may hold values from -6 to 6
- value_vectors: bfloat16 [2, 1024, 4096], P(None, 'tp', 'ep'), may hold values from -12 to 12
- cumulative_gate: float32 [2, 16, 4096], P(None, 'tp'), may hold values from -4096 to 0, as said below
- expert_input: bfloat16 [4096, 2048], P(('ep', 'tp')), may hold values from -6 to 6
- norm_gain: float32 [2048], replicated, may hold values from 0.1 to 1.9
- group_choice: int32 [4096], P(('ep', 'tp')), may hold values from 0 to 3, as said below
- group_weight: float32 [4096], P(('ep', 'tp')), may hold values from 0.3 to 1
- expert_logits: float32 [4096, 2], P(('ep', 'tp')), may hold values from -6 to 6
- gate_weight: bfloat16 [8, 2048, 2048], P('ep', 'tp'), may hold values from -0.125 to 0.125
- up_weight: bfloat16 [8, 2048, 2048], P('ep', 'tp'), may hold values from -0.125 to 0.125
- down_weight: bfloat16 [8, 2048, 2048], P('ep', 'tp'), may hold values from -0.25 to 0.25
Outputs:
- attention: bfloat16 [2, 1024, 4096], P(None, 'tp', 'ep')
- expert_output: bfloat16 [4096, 2048], P(('ep', 'tp'))
Inputs may be any that keep to these rules, and one draw needn't show every extreme that they name: `cumulative_gate`: each row is non-increasing along positions. `group_choice`: in each aligned block of 128 rows (the rows of one device) no group is named more than 40 times, and one group is named exactly 40 times in every block.
All inputs are finite; a program needn't handle non-finite values.
Results may differ from a plain program's by a relative error of at most 0.017.
Values may be sent and summed in bfloat16 or wider, within the bound.
A program may use at most 128 MiB of HBM per device.

v0:
```python
from functools import partial
import math

import jax
import jax.numpy as jnp
from jax import lax
from jax.sharding import PartitionSpec as P

neg_fill = -1e30
norm_eps = 1e-06


def partner(x, axis, distance):
    return lax.ppermute(x, axis, [(i, i ^ 1 << distance) for i in range(lax.axis_size(axis))])


def unchanged(running):
    return running


def attend(queries, key_vectors, value_vectors, cumulative_gate):
    seq_count, feat_width, seg_len = queries.shape
    heads_here = cumulative_gate.shape[1]
    head_dim = feat_width // heads_here
    half_len = seg_len // 2
    ep_size = lax.axis_size("ep")
    ep_rank = lax.axis_index("ep")
    score_scale = 1.0 / math.sqrt(head_dim)
    query_grid = queries.reshape(seq_count, heads_here, head_dim, seg_len)
    early_half = query_grid[:, :, :, :half_len]
    later_half = query_grid[:, :, :, half_len:]
    early_start = ep_rank * seg_len
    for bit_index in range(ep_size.bit_length() - 1):
        later_half = partner(later_half, "ep", bit_index)
    later_start = (ep_size - 1 - ep_rank) * seg_len + half_len
    halves = ((early_half, early_start), (later_half, later_start))
    query_gates = [
        lax.dynamic_slice_in_dim(cumulative_gate, early_start, half_len, 2),
        lax.dynamic_slice_in_dim(cumulative_gate, later_start, half_len, 2),
    ]

    def absorb(running, key_block, value_block, gate_block, key_start, half_index):
        query_block, query_start = halves[half_index]
        peak_old, total_old, acc_old = running
        scores = (
            jnp.einsum(
                "shdq,shdk->shqk", query_block, key_block, preferred_element_type=jnp.float32
            )
            * score_scale
        )
        scores = scores + query_gates[half_index][:, :, :, None] - gate_block[:, :, None, :]
        query_pos = query_start + jnp.arange(half_len, dtype=jnp.int32)
        key_pos = key_start + jnp.arange(key_block.shape[3], dtype=jnp.int32)
        allowed = key_pos[None, :] <= query_pos[:, None]
        scores = jnp.where(allowed, scores, neg_fill)
        peak_new = jnp.maximum(peak_old, jnp.max(scores, axis=3))
        shrink = jnp.exp(peak_old - peak_new)
        weights = jnp.where(allowed, jnp.exp(scores - peak_new[:, :, :, None]), 0.0)
        total_new = total_old * shrink + jnp.sum(weights, axis=3)
        acc_new = acc_old * shrink[:, :, None, :] + jnp.einsum(
            "shqk,shdk->shdq",
            weights.astype(jnp.bfloat16),
            value_block,
            preferred_element_type=jnp.float32,
        )
        return (peak_new, total_new, acc_new)

    blank_state = (
        jnp.full((seq_count, heads_here, half_len), neg_fill, jnp.float32),
        jnp.zeros((seq_count, heads_here, half_len), jnp.float32),
        jnp.zeros((seq_count, heads_here, head_dim, half_len), jnp.float32),
    )
    key_piece = lax.all_gather(key_vectors, "ep", axis=2, tiled=True)
    value_piece = lax.all_gather(value_vectors, "ep", axis=2, tiled=True)
    length = key_piece.shape[2]
    key_span = math.gcd(length, 1024)

    def visit_block(counter, inner):
        offset = counter * key_span
        key_block = lax.dynamic_slice_in_dim(key_piece, offset, key_span, 2).reshape(
            seq_count, heads_here, head_dim, key_span
        )
        value_block = lax.dynamic_slice_in_dim(value_piece, offset, key_span, 2).reshape(
            seq_count, heads_here, head_dim, key_span
        )
        gate_block = lax.dynamic_slice_in_dim(cumulative_gate, offset, key_span, 2)
        updated = []
        for half_index in range(2):
            last_pos = halves[half_index][1] + half_len - 1
            step_fn = partial(
                absorb,
                key_block=key_block,
                value_block=value_block,
                gate_block=gate_block,
                key_start=offset,
                half_index=half_index,
            )
            updated.append(lax.cond(offset <= last_pos, step_fn, unchanged, inner[half_index]))
        return tuple(updated)

    states = lax.fori_loop(0, length // key_span, visit_block, (blank_state, blank_state))
    outputs = []
    for half_index in range(2):
        acc_final = states[half_index][2]
        total_final = states[half_index][1]
        outputs.append((acc_final / total_final[:, :, None, :]).astype(jnp.bfloat16))
    later_out = outputs[1]
    for bit_index in range(ep_size.bit_length() - 1):
        later_out = partner(later_out, "ep", bit_index)
    return jnp.concatenate([outputs[0], later_out], axis=3).reshape(seq_count, feat_width, seg_len)


def expert_hidden(row_block, route_block, gate_weight, up_weight):
    gate_act = jnp.einsum("rd,efd->ref", row_block, gate_weight, preferred_element_type=jnp.float32)
    up_act = jnp.einsum("rd,efd->ref", row_block, up_weight, preferred_element_type=jnp.float32)
    return (jax.nn.silu(gate_act) * up_act * route_block.astype(jnp.float32)[:, :, None]).astype(
        jnp.bfloat16
    )


def mixture(
    expert_input,
    norm_gain,
    group_choice,
    group_weight,
    expert_logits,
    gate_weight,
    up_weight,
    down_weight,
):
    tok_rows, model_dim = expert_input.shape
    group_size = gate_weight.shape[0]
    ep_size = lax.axis_size("ep")
    capacity = 5 * tok_rows // (4 * ep_size)
    token_float = expert_input.astype(jnp.float32)
    normed = (
        token_float
        * lax.rsqrt(jnp.mean(token_float * token_float, axis=1, keepdims=True) + norm_eps)
        * norm_gain
    ).astype(jnp.bfloat16)
    routing = (group_weight[:, None] * jax.nn.softmax(expert_logits, axis=1)).astype(jnp.bfloat16)
    member = (group_choice[:, None] == jnp.arange(ep_size, dtype=jnp.int32)[None, :]).astype(
        jnp.int32
    )
    before = jnp.cumsum(member, axis=0) - member
    slot_index = jnp.sum(before * member, axis=1)
    flat_slot = group_choice * capacity + slot_index
    places = (
        flat_slot[None, :] == jnp.arange(ep_size * capacity, dtype=jnp.int32)[:, None]
    ).astype(jnp.bfloat16)
    outgoing = (
        jnp.dot(places, normed, preferred_element_type=jnp.float32)
        .astype(jnp.bfloat16)
        .reshape(ep_size, capacity, model_dim)
    )
    send_route = (
        jnp.dot(places, routing, preferred_element_type=jnp.float32)
        .astype(jnp.bfloat16)
        .reshape(ep_size, capacity, group_size)
    )
    arrived, arrived_route = (
        lax.all_to_all(outgoing, "ep", split_axis=0, concat_axis=0, tiled=True),
        lax.all_to_all(send_route, "ep", split_axis=0, concat_axis=0, tiled=True),
    )
    local_rows = arrived.reshape(ep_size * capacity, model_dim)
    local_route = arrived_route.reshape(ep_size * capacity, group_size)
    gathered_rows, gathered_route = (
        lax.all_gather(local_rows, "tp", axis=0, tiled=True),
        lax.all_gather(local_route, "tp", axis=0, tiled=True),
    )
    hidden = expert_hidden(gathered_rows, gathered_route, gate_weight, up_weight)
    summed = lax.psum_scatter(
        jnp.einsum("ref,efd->rd", hidden, down_weight, preferred_element_type=jnp.float32).astype(
            jnp.bfloat16
        ),
        "tp",
        scatter_dimension=0,
        tiled=True,
    )
    returned = lax.all_to_all(
        summed.reshape(ep_size, capacity, model_dim), "ep", split_axis=0, concat_axis=0, tiled=True
    )
    returned_flat = returned.reshape(ep_size * capacity, model_dim)
    return jnp.einsum(
        "pt,pd->td", places, returned_flat, preferred_element_type=jnp.float32
    ).astype(jnp.bfloat16)


def local(
    queries,
    key_vectors,
    value_vectors,
    cumulative_gate,
    expert_input,
    norm_gain,
    group_choice,
    group_weight,
    expert_logits,
    gate_weight,
    up_weight,
    down_weight,
):
    attention = attend(queries, key_vectors, value_vectors, cumulative_gate)
    expert_output = mixture(
        expert_input,
        norm_gain,
        group_choice,
        group_weight,
        expert_logits,
        gate_weight,
        up_weight,
        down_weight,
    )
    return (attention, expert_output)


def solution(mesh):
    return jax.shard_map(
        local,
        mesh=mesh,
        in_specs=(
            P(None, "tp", "ep"),
            P(None, "tp", "ep"),
            P(None, "tp", "ep"),
            P(None, "tp", None),
            P(("ep", "tp"), None),
            P(),
            P(("ep", "tp")),
            P(("ep", "tp")),
            P(("ep", "tp"), None),
            P("ep", "tp", None),
            P("ep", "tp", None),
            P("ep", "tp", None),
        ),
        out_specs=(P(None, "tp", "ep"), P(("ep", "tp"), None)),
        check_vma=False,
    )
```

profile of v0, /device:TPU:0, one launch (start us, length us, event | category | flops | bytes accessed | tf_op | source)
XLA Modules:
  0.0 254.1 jit_solution(3871763273252766201)
XLA Ops:
  7.2 1.4 fusion.43
  8.6 0.7 fusion.51
  9.5 0.8 select_reduce_fusion
  10.4 0.7 multiply_add_fusion.2
  11.0 1.4 convolution_convert_fusion
  12.5 15.0 %all_to_all.15 = bf16[4,40,2048]{2,1,0:T(8,128)(2,1)} all-to-all(bf16[4,40,2048]{2,1,0:T(8,128)(2,1)S(1)} %bitcast.57), channel_id=1, replica_groups=mesh['ep'=4,'tp'=8] {'ep'}, dimensions={0} | all-to-all | bytes 1310720 | tf_op jit(solution)/shard_map/all_to_all | solution.py:162
  27.6 0.7 all-gather.5.cloned.1.call-update
  28.3 0.7 all-gather.7.cloned.1.call-update
  29.1 0.7 reduce_max.27
  29.8 0.7 fusion.55
  30.5 0.8 convolution_convert_fusion.2
  31.4 7.0 %all_to_all.16 = bf16[4,40,2]{1,2,0:T(2,128)(2,1)S(1)} all-to-all(bf16[4,40,2]{1,2,0:T(2,128)(2,1)S(1)} %copy.19), channel_id=1, replica_groups=mesh['ep'=4,'tp'=8] {'ep'}, dimensions={0} | all-to-all | bytes 1280 | tf_op jit(solution)/shard_map/all_to_all | solution.py:163
  38.5 12.6 %all-gather = bf16[8,160,2]{1,2,0:T(2,128)(2,1)S(1)} all-gather(bf16[1,160,2]{1,2,0:T(2,128)(2,1)S(1)} %reshape.97), channel_id=1, replica_groups=mesh['ep'=4,'tp'=8] {'tp'}, dimensions={0}, use_global_device_ids=true | all-gather | bytes 5760 | tf_op jit(solution)/shard_map/all_gather | solution.py:169
  51.2 32.3 %all-gather.9.cloned.1.call-done = bf16[1280,2048]{1,0:T(8,128)(2,1)} async-done(((bf16[160,2048]{1,0:T(8,128)(2,1)}), bf16[1280,2048]{1,0:T(8,128)(2,1)}) %all-gather.9.cloned.1.call-update) | async-done | bytes 5242896 | tf_op jit(solution)/shard_map/all_gather | solution.py:168
  83.4 7.6 %fusion.32 = f32[1280,2,256]{2,0,1:T(8,128)} fusion(bf16[2,256,2048]{2,1,0:T(8,128)(2,1)} %param.27, bf16[1280,2048]{1,0:T(8,128)(2,1)} %all-gather.9.cloned.1.call-done), kind=kOutput, calls=%fused_computation.40 | convolution fusion | flops 2684354560 | bytes 9961472 | tf_op jit(solution)/shard_map/rd,efd->ref/dot_general | solution.py:114
  91.1 10.7 %bitcast_convert_fusion = bf16[1280,2048]{1,0:T(8,128)(2,1)} fusion(bf16[2,256,2048]{2,1,0:T(8,128)(2,1)S(1)} %copy-done, bf16[2,256,2048]{2,1,0:T(8,128)(2,1)} %param.28, bf16[1280,2048]{1,0:T(8,128)(2,1)} %all-gather.9.cloned.1.call-done, f32[1280,2,256]{2,0,1:T(8,128)} %fusion.32, f32[1280,2]{0,1:T(2,128)S(1)} %reshape.99), kind=kOutput, calls=%fused_computation.37 | convolution fusion | flops 5375918080 | bytes 17311744 | tf_op jit(solution)/shard_map/ref,efd->rd/dot_general | solution.py:173
  101.9 1.6 collective-permute-start
  103.5 10.5 %collective-permute-done = bf16[2,2,64,512]{3,2,1,0:T(8,128)(2,1)S(1)} collective-permute-done((bf16[2,2,64,512]{3,2,1,0:T(8,128)(2,1)S(1)}, bf16[2,2,64,512]{3,2,1,0:T(8,128)(2,1)S(1)}, u32[]{:S(2)}, u32[]{:S(2)}) %collective-permute-start) | collective-permute-done | bytes 262176 | tf_op jit(solution)/shard_map/ppermute | solution.py:14
  114.0 1.3 collective-permute-start.1
  115.3 9.3 %collective-permute-done.1 = bf16[2,2,64,512]{3,2,1,0:T(8,128)(2,1)} collective-permute-done((bf16[2,2,64,512]{3,2,1,0:T(8,128)(2,1)S(1)}, bf16[2,2,64,512]{3,2,1,0:T(8,128)(2,1)}, u32[]{:S(2)}, u32[]{:S(2)}) %collective-permute-start.1) | collective-permute-done | bytes 262176 | tf_op jit(solution)/shard_map/ppermute | solution.py:14
  124.6 37.3 %all-gather.7.cloned.1.call-done = bf16[2,128,4096]{2,1,0:T(8,128)(2,1)} async-done(((bf16[2,128,1024]{2,1,0:T(8,128)(2,1)}), bf16[2,128,4096]{2,1,0:T(8,128)(2,1)}) %all-gather.7.cloned.1.call-update) | async-done | bytes 2097168 | tf_op jit(solution)/shard_map/all_gather | solution.py:74
  161.9 0.9 broadcast_in_dim.42
  162.8 0.9 broadcast_in_dim.42.clone
  163.6 62.2 %while.26 = (s32[]{:T(128)}, f32[2,2,512]{2,1,0:T(2,128)S(1)}, f32[2,2,512]{2,1,0:T(2,128)S(1)}, f32[2,2,64,512]{3,2,1,0:T(8,128)}, f32[2,2,512]{2,1,0:T(2,128)S...) while((s32[]{:T(128)}, f32[2,2,512]{2,1,0:T(2,128)S(1)}, ...), condition=%wide.region_9.10_spmd, body=%wide.region_0.9_spmd.sunk | while | flops 1155017728 | bytes 70197928 | solution.py:101
  163.6 1.3 constant_dynamic-slice_fusion.7
  165.0 10.4 %conditional.4 = ((f32[2,2,512]{2,1,0:T(2,128)S(1)}, f32[2,2,512]{2,1,0:T(2,128)S(1)}, f32[2,2,64,512]{3,2,1,0:T(8,128)})) conditional(s32[]{:T(128)} %convert_element_type.116, (f32[2,2,512]{2,1,0:T(2,128)S(1)}, f32[2,2,512]{2,1,0:T(2,128)S(1)}, f32[2,2,64,512]{3,2,1,0:T(8,128)}) %tuple.69, (s32[]{:T(128)}, s32[]{:T(128)}, ...), branch_computations={%region_1.0_spmd, %region_2.4_spmd} | conditional | flops 577508864 | bytes 34033760 | solution.py:98
  165.0 0.4 broadcast_compare_fusion
  165.4 2.5 fusion.2
  167.9 3.5 %fusion.1 = f32[2,2,512]{2,1,0:T(2,128)S(1)} fusion(f32[2,2,512,1024]{3,2,1,0:T(8,128)S(1)} %get-tuple-element.576, f32[2,2,512]{2,1,0:T(2,128)S(1)} %max.0, f32[2,2,1024]{2,1,0:T(2,128)S(1)} %get-tuple-element.486, f32[2,2,512]{2,1,0:T(2,128)S(1)} %get-tuple-element.485, pred[512,1024]{1,0:T(8,128)(4,1)S(1)} %broadcast_compare_fusion), kind=kLoop, calls=%fused_computation.3 | loop fusion | flops 14678016 | bytes 8953856 | tf_op jit(solution)/shard_map/while/body/eval_jaxpr/cond/branch_1_fun/reduce_sum | solution.py:59
  171.5 3.1 %fusion.9 = f32[2,2,64,512]{3,2,1,0:T(8,128)S(1)} fusion(bf16[2,2,64,1024]{3,2,1,0:T(8,128)(2,1)S(1)} %get-tuple-element.489, f32[2,2,512,1024]{3,2,1,0:T(8,128)S(1)} %get-tuple-element.576, f32[2,2,512]{2,1,0:T(2,128)S(1)} %max.0, f32[2,2,1024]{2,1,0:T(2,128)S(1)} %get-tuple-element.486, f32[2,2,512]{2,1,0:T(2,128)S(1)} %get-tuple-element.485, ...), kind=kOutput, calls=%fused_computation.8 | convolution fusion | flops 283377664 | bytes 10526720 | tf_op jit(solution)/shard_map/while/body/eval_jaxpr/cond/branch_1_fun/shqk,shdk->shdq/dot_general | solution.py:60
  174.6 0.8 copy-done.2
  175.4 11.6 %conditional.5 = ((f32[2,2,512]{2,1,0:T(2,128)S(1)}, f32[2,2,512]{2,1,0:T(2,128)S(1)}, f32[2,2,64,512]{3,2,1,0:T(8,128)})) conditional(s32[]{:T(128)} %convert_element_type.117, (f32[2,2,512]{2,1,0:T(2,128)S(1)}, f32[2,2,512]{2,1,0:T(2,128)S(1)}, f32[2,2,64,512]{3,2,1,0:T(8,128)}) %tuple.71, (s32[]{:T(128)}, s32[]{:T(128)}, ...), branch_computations={%region_5.5_spmd, %region_6.8_spmd} | conditional | flops 577508864 | bytes 34033760 | solution.py:98
  175.4 0.4 broadcast_compare_fusion.1
  175.8 3.6 %fusion.17 = (f32[2,2,512]{2,1,0:T(2,128)S(1)}, f32[2,2,512,1024]{3,2,1,0:T(8,128)S(1)}) fusion(f32[2,2,1024]{2,1,0:T(2,128)S(1)} %get-tuple-element.496, f32[2,2,512]{2,1,0:T(2,128)S(1)} %get-tuple-element.495, pred[512,1024]{1,0:T(8,128)(4,1)S(1)} %broadcast_compare_fusion.1, bf16[2,2,64,512]{3,2,1,0:T(8,128)(2,1)} %get-tuple-element.493, ...), kind=kOutput, calls=%fused_computation.21 | convolution fusion | flops 278919168 | bytes 9732096 | tf_op jit(solution)/shard_map/while/body/eval_jaxpr/cond/branch_1_fun/shdq,shdk->shqk/dot_general | solution.py:46
  179.4 3.5 %fusion.16 = f32[2,2,512]{2,1,0:T(2,128)S(1)} fusion(f32[2,2,512,1024]{3,2,1,0:T(8,128)S(1)} %get-tuple-element.578, f32[2,2,512]{2,1,0:T(2,128)S(1)} %max.5, f32[2,2,1024]{2,1,0:T(2,128)S(1)} %get-tuple-element.496, f32[2,2,512]{2,1,0:T(2,128)S(1)} %get-tuple-element.495, pred[512,1024]{1,0:T(8,128)(4,1)S(1)} %broadcast_compare_fusion.1), kind=kLoop, calls=%fused_computation.20 | loop fusion | flops 14678016 | bytes 8953856 | tf_op jit(solution)/shard_map/while/body/eval_jaxpr/cond/branch_1_fun/reduce_sum | solution.py:59
  183.0 3.1 %fusion.24 = f32[2,2,64,512]{3,2,1,0:T(8,128)S(1)} fusion(bf16[2,2,64,1024]{3,2,1,0:T(8,128)(2,1)S(1)} %get-tuple-element.499, f32[2,2,512,1024]{3,2,1,0:T(8,128)S(1)} %get-tuple-element.578, f32[2,2,512]{2,1,0:T(2,128)S(1)} %max.5, f32[2,2,1024]{2,1,0:T(2,128)S(1)} %get-tuple-element.496, f32[2,2,512]{2,1,0:T(2,128)S(1)} %get-tuple-element.495, ...), kind=kOutput, calls=%fused_computation.25 | convolution fusion | flops 283377664 | bytes 10526720 | tf_op jit(solution)/shard_map/while/body/eval_jaxpr/cond/branch_1_fun/shqk,shdk->shdq/dot_general | solution.py:60
  186.2 0.8 copy-done.4
  186.9 1.3 constant_dynamic-slice_fusion.7
  188.3 11.6 %conditional.5 = ((f32[2,2,512]{2,1,0:T(2,128)S(1)}, f32[2,2,512]{2,1,0:T(2,128)S(1)}, f32[2,2,64,512]{3,2,1,0:T(8,128)})) conditional(s32[]{:T(128)} %convert_element_type.117, (f32[2,2,512]{2,1,0:T(2,128)S(1)}, f32[2,2,512]{2,1,0:T(2,128)S(1)}, f32[2,2,64,512]{3,2,1,0:T(8,128)}) %tuple.71, (s32[]{:T(128)}, s32[]{:T(128)}, ...), branch_computations={%region_5.5_spmd, %region_6.8_spmd} | conditional | flops 577508864 | bytes 34033760 | solution.py:98
  188.4 0.4 broadcast_compare_fusion.1
  188.7 3.6 %fusion.17 = (f32[2,2,512]{2,1,0:T(2,128)S(1)}, f32[2,2,512,1024]{3,2,1,0:T(8,128)S(1)}) fusion(f32[2,2,1024]{2,1,0:T(2,128)S(1)} %get-tuple-element.496, f32[2,2,512]{2,1,0:T(2,128)S(1)} %get-tuple-element.495, pred[512,1024]{1,0:T(8,128)(4,1)S(1)} %broadcast_compare_fusion.1, bf16[2,2,64,512]{3,2,1,0:T(8,128)(2,1)} %get-tuple-element.493, ...), kind=kOutput, calls=%fused_computation.21 | convolution fusion | flops 278919168 | bytes 9732096 | tf_op jit(solution)/shard_map/while/body/eval_jaxpr/cond/branch_1_fun/shdq,shdk->shqk/dot_general | solution.py:46
  192.4 3.5 %fusion.16 = f32[2,2,512]{2,1,0:T(2,128)S(1)} fusion(f32[2,2,512,1024]{3,2,1,0:T(8,128)S(1)} %get-tuple-element.578, f32[2,2,512]{2,1,0:T(2,128)S(1)} %max.5, f32[2,2,1024]{2,1,0:T(2,128)S(1)} %get-tuple-element.496, f32[2,2,512]{2,1,0:T(2,128)S(1)} %get-tuple-element.495, pred[512,1024]{1,0:T(8,128)(4,1)S(1)} %broadcast_compare_fusion.1), kind=kLoop, calls=%fused_computation.20 | loop fusion | flops 14678016 | bytes 8953856 | tf_op jit(solution)/shard_map/while/body/eval_jaxpr/cond/branch_1_fun/reduce_sum | solution.py:59
  196.0 3.1 %fusion.24 = f32[2,2,64,512]{3,2,1,0:T(8,128)S(1)} fusion(bf16[2,2,64,1024]{3,2,1,0:T(8,128)(2,1)S(1)} %get-tuple-element.499, f32[2,2,512,1024]{3,2,1,0:T(8,128)S(1)} %get-tuple-element.578, f32[2,2,512]{2,1,0:T(2,128)S(1)} %max.5, f32[2,2,1024]{2,1,0:T(2,128)S(1)} %get-tuple-element.496, f32[2,2,512]{2,1,0:T(2,128)S(1)} %get-tuple-element.495, ...), kind=kOutput, calls=%fused_computation.25 | convolution fusion | flops 283377664 | bytes 10526720 | tf_op jit(solution)/shard_map/while/body/eval_jaxpr/cond/branch_1_fun/shqk,shdk->shdq/dot_general | solution.py:60
  199.1 0.8 copy-done.4
  199.9 1.3 constant_dynamic-slice_fusion.7
  201.3 11.6 %conditional.5 = ((f32[2,2,512]{2,1,0:T(2,128)S(1)}, f32[2,2,512]{2,1,0:T(2,128)S(1)}, f32[2,2,64,512]{3,2,1,0:T(8,128)})) conditional(s32[]{:T(128)} %convert_element_type.117, (f32[2,2,512]{2,1,0:T(2,128)S(1)}, f32[2,2,512]{2,1,0:T(2,128)S(1)}, f32[2,2,64,512]{3,2,1,0:T(8,128)}) %tuple.71, (s32[]{:T(128)}, s32[]{:T(128)}, ...), branch_computations={%region_5.5_spmd, %region_6.8_spmd} | conditional | flops 577508864 | bytes 34033760 | solution.py:98
  201.3 0.4 broadcast_compare_fusion.1
  201.7 3.6 %fusion.17 = (f32[2,2,512]{2,1,0:T(2,128)S(1)}, f32[2,2,512,1024]{3,2,1,0:T(8,128)S(1)}) fusion(f32[2,2,1024]{2,1,0:T(2,128)S(1)} %get-tuple-element.496, f32[2,2,512]{2,1,0:T(2,128)S(1)} %get-tuple-element.495, pred[512,1024]{1,0:T(8,128)(4,1)S(1)} %broadcast_compare_fusion.1, bf16[2,2,64,512]{3,2,1,0:T(8,128)(2,1)} %get-tuple-element.493, ...), kind=kOutput, calls=%fused_computation.21 | convolution fusion | flops 278919168 | bytes 9732096 | tf_op jit(solution)/shard_map/while/body/eval_jaxpr/cond/branch_1_fun/shdq,shdk->shqk/dot_general | solution.py:46
  205.3 3.5 %fusion.16 = f32[2,2,512]{2,1,0:T(2,128)S(1)} fusion(f32[2,2,512,1024]{3,2,1,0:T(8,128)S(1)} %get-tuple-element.578, f32[2,2,512]{2,1,0:T(2,128)S(1)} %max.5, f32[2,2,1024]{2,1,0:T(2,128)S(1)} %get-tuple-element.496, f32[2,2,512]{2,1,0:T(2,128)S(1)} %get-tuple-element.495, pred[512,1024]{1,0:T(8,128)(4,1)S(1)} %broadcast_compare_fusion.1), kind=kLoop, calls=%fused_computation.20 | loop fusion | flops 14678016 | bytes 8953856 | tf_op jit(solution)/shard_map/while/body/eval_jaxpr/cond/branch_1_fun/reduce_sum | solution.py:59
  208.9 3.1 %fusion.24 = f32[2,2,64,512]{3,2,1,0:T(8,128)S(1)} fusion(bf16[2,2,64,1024]{3,2,1,0:T(8,128)(2,1)S(1)} %get-tuple-element.499, f32[2,2,512,1024]{3,2,1,0:T(8,128)S(1)} %get-tuple-element.578, f32[2,2,512]{2,1,0:T(2,128)S(1)} %max.5, f32[2,2,1024]{2,1,0:T(2,128)S(1)} %get-tuple-element.496, f32[2,2,512]{2,1,0:T(2,128)S(1)} %get-tuple-element.495, ...), kind=kOutput, calls=%fused_computation.25 | convolution fusion | flops 283377664 | bytes 10526720 | tf_op jit(solution)/shard_map/while/body/eval_jaxpr/cond/branch_1_fun/shqk,shdk->shdq/dot_general | solution.py:60
  212.1 0.8 copy-done.4
  212.8 1.3 constant_dynamic-slice_fusion.7
  214.2 11.6 %conditional.5 = ((f32[2,2,512]{2,1,0:T(2,128)S(1)}, f32[2,2,512]{2,1,0:T(2,128)S(1)}, f32[2,2,64,512]{3,2,1,0:T(8,128)})) conditional(s32[]{:T(128)} %convert_element_type.117, (f32[2,2,512]{2,1,0:T(2,128)S(1)}, f32[2,2,512]{2,1,0:T(2,128)S(1)}, f32[2,2,64,512]{3,2,1,0:T(8,128)}) %tuple.71, (s32[]{:T(128)}, s32[]{:T(128)}, ...), branch_computations={%region_5.5_spmd, %region_6.8_spmd} | conditional | flops 577508864 | bytes 34033760 | solution.py:98
  214.6 3.6 %fusion.17 = (f32[2,2,512]{2,1,0:T(2,128)S(1)}, f32[2,2,512,1024]{3,2,1,0:T(8,128)S(1)}) fusion(f32[2,2,1024]{2,1,0:T(2,128)S(1)} %get-tuple-element.496, f32[2,2,512]{2,1,0:T(2,128)S(1)} %get-tuple-element.495, pred[512,1024]{1,0:T(8,128)(4,1)S(1)} %broadcast_compare_fusion.1, bf16[2,2,64,512]{3,2,1,0:T(8,128)(2,1)} %get-tuple-element.493, ...), kind=kOutput, calls=%fused_computation.21 | convolution fusion | flops 278919168 | bytes 9732096 | tf_op jit(solution)/shard_map/while/body/eval_jaxpr/cond/branch_1_fun/shdq,shdk->shqk/dot_general | solution.py:46
  218.3 3.5 %fusion.16 = f32[2,2,512]{2,1,0:T(2,128)S(1)} fusion(f32[2,2,512,1024]{3,2,1,0:T(8,128)S(1)} %get-tuple-element.578, f32[2,2,512]{2,1,0:T(2,128)S(1)} %max.5, f32[2,2,1024]{2,1,0:T(2,128)S(1)} %get-tuple-element.496, f32[2,2,512]{2,1,0:T(2,128)S(1)} %get-tuple-element.495, pred[512,1024]{1,0:T(8,128)(4,1)S(1)} %broadcast_compare_fusion.1), kind=kLoop, calls=%fused_computation.20 | loop fusion | flops 14678016 | bytes 8953856 | tf_op jit(solution)/shard_map/while/body/eval_jaxpr/cond/branch_1_fun/reduce_sum | solution.py:59
  221.9 3.1 %fusion.24 = f32[2,2,64,512]{3,2,1,0:T(8,128)S(1)} fusion(bf16[2,2,64,1024]{3,2,1,0:T(8,128)(2,1)S(1)} %get-tuple-element.499, f32[2,2,512,1024]{3,2,1,0:T(8,128)S(1)} %get-tuple-element.578, f32[2,2,512]{2,1,0:T(2,128)S(1)} %max.5, f32[2,2,1024]{2,1,0:T(2,128)S(1)} %get-tuple-element.496, f32[2,2,512]{2,1,0:T(2,128)S(1)} %get-tuple-element.495, ...), kind=kOutput, calls=%fused_computation.25 | convolution fusion | flops 283377664 | bytes 10526720 | tf_op jit(solution)/shard_map/while/body/eval_jaxpr/cond/branch_1_fun/shqk,shdk->shdq/dot_general | solution.py:60
  225.0 0.8 copy-done.4
  225.8 1.1 divide_convert_fusion
  227.3 3.5 %all-to-all-start.2 = ((bf16[4,40,2048]{2,1,0:T(8,128)(2,1)}), bf16[4,40,2048]{2,1,0:T(8,128)(2,1)S(1)}, u32[]{:S(2)}, u32[]{:S(2)}) async-start(bf16[4,40,2048]{2,1,0:T(8,128)(2,1)} %bitcast.58), calls=%async_computation.3 | async-start | bytes 1310720 | tf_op jit(solution)/shard_map/all_to_all | solution.py:180
  230.7 5.4 %collective-permute-done.2 = bf16[2,2,64,512]{3,2,1,0:T(8,128)(2,1)S(1)} collective-permute-done((bf16[2,2,64,512]{3,2,1,0:T(8,128)(2,1)S(1)}, bf16[2,2,64,512]{3,2,1,0:T(8,128)(2,1)S(1)}, u32[]{:S(2)}, u32[]{:S(2)}) %collective-permute-start.2) | collective-permute-done | bytes 262176 | tf_op jit(solution)/shard_map/ppermute | solution.py:14
  236.1 1.1 divide_convert_fusion.1
  237.2 8.3 %collective-permute-done.3 = bf16[2,2,64,512]{3,2,1,0:T(8,128)(2,1)S(1)} collective-permute-done((bf16[2,2,64,512]{3,2,1,0:T(8,128)(2,1)S(1)}, bf16[2,2,64,512]{3,2,1,0:T(8,128)(2,1)S(1)}, u32[]{:S(2)}, u32[]{:S(2)}) %collective-permute-start.3) | collective-permute-done | bytes 262176 | tf_op jit(solution)/shard_map/ppermute | solution.py:14
  245.6 0.9 pad_maximum_fusion
  246.4 1.1 convolution_convert_fusion.1
  (83 shorter events, 1.8 us)
Async XLA Ops:
  7.2 83.9 %copy-start = (bf16[2,256,2048]{2,1,0:T(8,128)(2,1)S(1)}, bf16[2,256,2048]{2,1,0:T(8,128)(2,1)}, u32[]{:S(2)}) copy-start(bf16[2,256,2048]{2,1,0:T(8,128)(2,1)} %param.29) | copy-start | bytes 6291460
  7.2 76.3 %all-gather.9.cloned.1.call-start = ((), (), s32[]{:S(2)}) async-start(), calls=%async_computation.6 | async-start | bytes 5898240 | tf_op jit(solution)/shard_map/all_gather | solution.py:168
  11.0 19.4 %copy-start.7 = (s32[128]{0:T(128)}, s32[128]{0:T(128)S(1)}, u32[]{:S(2)}) copy-start(s32[128]{0:T(128)S(1)} %multiply_add_fusion.2) | copy-start | bytes 1540
  27.5 97.1 %all-gather.5.cloned.1.call-start = ((), (), s32[]{:S(2)}) async-start(), calls=%async_computation.4 | async-start | bytes 2621440 | tf_op jit(solution)/shard_map/all_gather | solution.py:73
  28.3 133.6 %all-gather.7.cloned.1.call-start = ((), (), s32[]{:S(2)}) async-start(), calls=%async_computation.5 | async-start | bytes 2621440 | tf_op jit(solution)/shard_map/all_gather | solution.py:74
  29.0 198.2 %reduce-scatter.2.cloned.1.call-start = ((), (), s32[]{:S(2)}) async-start(), calls=%async_computation.7 | async-start | bytes 5898240 | tf_op jit(solution)/shard_map/reduce_scatter | solution.py:172
  91.1 10.8 %copy-start.5 = (bf16[2,128,1024]{2,1,0:T(8,128)(2,1)S(1)}, bf16[2,128,1024]{2,1,0:T(8,128)(2,1)}, u32[]{:S(2)}) copy-start(bf16[2,128,1024]{2,1,0:T(8,128)(2,1)} %param.18) | copy-start | bytes 1572868
  91.1 24.2 %copy-start.6 = (f32[2,2,4096]{2,1,0:T(2,128)S(1)}, f32[2,2,4096]{2,1,0:T(2,128)}, u32[]{:S(2)}) copy-start(f32[2,2,4096]{2,1,0:T(2,128)} %param.21) | copy-start | bytes 196612
  101.9 12.1 %collective-permute-start = (bf16[2,2,64,512]{3,2,1,0:T(8,128)(2,1)S(1)}, bf16[2,2,64,512]{3,2,1,0:T(8,128)(2,1)S(1)}, u32[]{:S(2)}, u32[]{:S(2)}) collective-permute-start(bf16[2,2,64,512]{3,2,1,0:T(8,128)(2,1)S(1)} %get-tuple-element.581), channel_id=1, source_target_pairs={{0,8},{8,0},{16,24},{24,16},{1,9},{9,1},{17,25},{25,17},{2,10},{10... | collective-permute-start | bytes 786440 | tf_op jit(solution)/shard_map/ppermute | solution.py:14
  114.0 10.6 %collective-permute-start.1 = (bf16[2,2,64,512]{3,2,1,0:T(8,128)(2,1)S(1)}, bf16[2,2,64,512]{3,2,1,0:T(8,128)(2,1)}, u32[]{:S(2)}, u32[]{:S(2)}) collective-permute-start(bf16[2,2,64,512]{3,2,1,0:T(8,128)(2,1)S(1)} %collective-permute-done), channel_id=1, source_target_pairs={{0,16},{8,24},{16,0},{24,8},{1,17},{9,25},{17,1},{25,9},{2,18},{10... | collective-permute-start | bytes 786440 | tf_op jit(solution)/shard_map/ppermute | solution.py:14
  163.6 82.8 %copy-start.8 = (s32[128]{0:T(128)S(1)}, s32[128]{0:T(128)}, u32[]{:S(2)}) copy-start(s32[128]{0:T(128)} %copy-done.7) | copy-start | bytes 1540
  165.4 6.1 %copy-start.1 = (f32[2,2,64,512]{3,2,1,0:T(8,128)S(1)}, f32[2,2,64,512]{3,2,1,0:T(8,128)}, u32[]{:S(2)}) copy-start(f32[2,2,64,512]{3,2,1,0:T(8,128)} %get-tuple-element.488) | copy-start | bytes 1572868 | tf_op jit(solution)/shard_map/while/body/eval_jaxpr/cond
  174.6 0.8 copy-start.2
  175.8 7.3 %copy-start.3 = (f32[2,2,64,512]{3,2,1,0:T(8,128)S(1)}, f32[2,2,64,512]{3,2,1,0:T(8,128)}, u32[]{:S(2)}) copy-start(f32[2,2,64,512]{3,2,1,0:T(8,128)} %get-tuple-element.498) | copy-start | bytes 1572868 | tf_op jit(solution)/shard_map/while/body/eval_jaxpr/cond
  186.2 0.8 copy-start.4
  188.7 7.3 %copy-start.3 = (f32[2,2,64,512]{3,2,1,0:T(8,128)S(1)}, f32[2,2,64,512]{3,2,1,0:T(8,128)}, u32[]{:S(2)}) copy-start(f32[2,2,64,512]{3,2,1,0:T(8,128)} %get-tuple-element.498) | copy-start | bytes 1572868 | tf_op jit(solution)/shard_map/while/body/eval_jaxpr/cond
  199.1 0.8 copy-start.4
  201.7 7.2 %copy-start.3 = (f32[2,2,64,512]{3,2,1,0:T(8,128)S(1)}, f32[2,2,64,512]{3,2,1,0:T(8,128)}, u32[]{:S(2)}) copy-start(f32[2,2,64,512]{3,2,1,0:T(8,128)} %get-tuple-element.498) | copy-start | bytes 1572868 | tf_op jit(solution)/shard_map/while/body/eval_jaxpr/cond
  212.0 0.8 copy-start.4
  214.6 7.3 %copy-start.3 = (f32[2,2,64,512]{3,2,1,0:T(8,128)S(1)}, f32[2,2,64,512]{3,2,1,0:T(8,128)}, u32[]{:S(2)}) copy-start(f32[2,2,64,512]{3,2,1,0:T(8,128)} %get-tuple-element.498) | copy-start | bytes 1572868 | tf_op jit(solution)/shard_map/while/body/eval_jaxpr/cond
  225.0 0.8 copy-start.4
  226.9 9.2 %collective-permute-start.2 = (bf16[2,2,64,512]{3,2,1,0:T(8,128)(2,1)S(1)}, bf16[2,2,64,512]{3,2,1,0:T(8,128)(2,1)S(1)}, u32[]{:S(2)}, u32[]{:S(2)}) collective-permute-start(bf16[2,2,64,512]{3,2,1,0:T(8,128)(2,1)S(1)} %divide_convert_fusion), channel_id=1, source_target_pairs={{0,8},{8,0},{16,24},{24,16},{1,9},{9,1},{17,25},{25,17},{2,10},{10... | collective-permute-start | bytes 786440 | tf_op jit(solution)/shard_map/ppermute | solution.py:14
  227.3 19.2 %all-to-all-start.2 = ((bf16[4,40,2048]{2,1,0:T(8,128)(2,1)}), bf16[4,40,2048]{2,1,0:T(8,128)(2,1)S(1)}, u32[]{:S(2)}, u32[]{:S(2)}) async-start(bf16[4,40,2048]{2,1,0:T(8,128)(2,1)} %bitcast.58), calls=%async_computation.3 | async-start | bytes 1310720 | tf_op jit(solution)/shard_map/all_to_all | solution.py:180
  236.1 9.4 %collective-permute-start.3 = (bf16[2,2,64,512]{3,2,1,0:T(8,128)(2,1)S(1)}, bf16[2,2,64,512]{3,2,1,0:T(8,128)(2,1)S(1)}, u32[]{:S(2)}, u32[]{:S(2)}) collective-permute-start(bf16[2,2,64,512]{3,2,1,0:T(8,128)(2,1)S(1)} %collective-permute-done.2), channel_id=1, source_target_pairs={{0,16},{8,24},{16,0},{24,8},{1,17},{9,25},{17,1},{25,9},{2,18},{10... | collective-permute-start | bytes 786440 | tf_op jit(solution)/shard_map/ppermute | solution.py:14
Sparse Core Ops, SparseCore 0:
  27.6 55.7 all-gather.8
  85.3 37.5 all-gather.4
  124.7 37.1 all-gather.6
  164.1 59.8 reduce-scatter.1
where the time goes:
time: 255 us; the launch traced here: 254 us
  waiting for transfers between devices  105 us (41%)
  matrix products  54.4 us (21%)
  blocking collectives  34.6 us (14%)
  other arithmetic  27.9 us (11%)
  between operations  13.8 us (5%)
  local copies, waits for them, and re-layouts  11.3 us (4%)
  starting transfers between devices  6.89 us (3%)
    all_gather x1, waiting for transfers between devices, attend(): value_piece = lax.all_gather(value_vectors, 'ep', axis=2, tiled=True)  37.3 us
    ppermute x4, waiting for transfers between devices, partner(): lax.ppermute(x, axis, [(i, i ^ 1 << distance) for i in range(lax.axis_siz...  33.6 us
    all_gather x1, waiting for transfers between devices, mixture(): lax.all_gather(local_rows, 'tp', axis=0, tiled=True)  32.3 us
    reduce_sum x5, other arithmetic, absorb(): total_new = total_old * shrink + jnp.sum(weights, axis=3)  17.7 us
    dot_general x5, matrix products, absorb(): jnp.einsum('shdq,shdk->shqk', query_block, key_block, preferred_element_t...  17 us
    dot_general x5, matrix products, absorb(): jnp.einsum('shqk,shdk->shdq', weights.astype(jnp.bfloat16), value_block,...  15.6 us
    all_to_all x1, blocking collectives, mixture(): lax.all_to_all(outgoing, 'ep', split_axis=0, concat_axis=0, tiled=True)  15 us
    all_gather x1, blocking collectives, mixture(): lax.all_gather(local_route, 'tp', axis=0, tiled=True)  12.6 us
  transfers between devices with their start and end apart: 9, of which 6 were waited for; matrix products, arithmetic and copies ran while one was open for 33% of the time, Pallas kernels for 0%

commit v1 on v0

--- a/solution.py
+++ b/solution.py
@@ -4,6 +4,8 @@
 import jax
 import jax.numpy as jnp
 from jax import lax
+from jax.experimental import pallas as pl
+from jax.experimental.pallas import tpu as pltpu
 from jax.sharding import PartitionSpec as P
 
 neg_fill = -1e30
@@ -108,6 +110,148 @@
     for bit_index in range(ep_size.bit_length() - 1):
         later_out = partner(later_out, "ep", bit_index)
     return jnp.concatenate([outputs[0], later_out], axis=3).reshape(seq_count, feat_width, seg_len)
+
+
+def gate_rows(gate, sign, first):
+    part_a = gate.astype(jnp.bfloat16).astype(jnp.float32)
+    rest = gate - part_a
+    part_b = rest.astype(jnp.bfloat16).astype(jnp.float32)
+    part_c = rest - part_b
+    row = lax.broadcasted_iota(jnp.int32, (16, gate.shape[1]), 0)
+    ones = jnp.where((row >= 3 - first) & (row < 6 - first), 1.0, 0.0)
+    rows = jnp.where(row == first, sign * part_a, ones)
+    rows = jnp.where(row == first + 1, sign * part_b, rows)
+    return jnp.where(row == first + 2, sign * part_c, rows)
+
+
+def attend_pair(head_dim, seg_len, seg_count, load, gate_of, store, keys_t, queries_x, values_x, acc, peak):
+    scale = 1.0 / math.sqrt(head_dim)
+    chunk = min(256, seg_len)
+    depth = head_dim + 16
+
+    def fill(block, _):
+        gate = gate_of(block)
+        local_gate = gate - gate[:, :1]
+        at = pl.multiple_of(block * seg_len, seg_len)
+        key_rows = jnp.concatenate(
+            [load(1, block).astype(jnp.float32), gate_rows(local_gate, -1.0, 0)], axis=0
+        )
+        keys_t[pl.ds(at, seg_len), :] = jnp.transpose(key_rows).astype(jnp.bfloat16)
+        query_rows = jnp.concatenate(
+            [load(0, block).astype(jnp.float32) * scale, gate_rows(local_gate, 1.0, 3)], axis=0
+        )
+        queries_x[block] = query_rows.astype(jnp.bfloat16)
+        values_x[block, :head_dim, :] = load(2, block)
+        values_x[block, head_dim:, :] = jnp.ones((16, seg_len), jnp.bfloat16)
+        return 0
+
+    lax.fori_loop(0, seg_count, fill, 0)
+
+    def query_step(block, _):
+        base = gate_of(block)[:, :1]
+        at = pl.multiple_of(block * seg_len, seg_len)
+        for c in range(seg_len // chunk):
+            cols = slice(c * chunk, (c + 1) * chunk)
+            span = (c + 1) * chunk
+            scores = jnp.dot(
+                keys_t[pl.ds(at, span), :],
+                queries_x[block, :, cols],
+                preferred_element_type=jnp.float32,
+            )
+            key_pos = lax.broadcasted_iota(jnp.int32, (span, chunk), 0)
+            query_pos = c * chunk + lax.broadcasted_iota(jnp.int32, (span, chunk), 1)
+            scores = jnp.where(key_pos <= query_pos, scores, neg_fill)
+            top = jnp.max(scores, axis=0, keepdims=True)
+            weights = jnp.exp(scores - top).astype(jnp.bfloat16)
+            peak[:, cols] = top
+            acc[:, cols] = jnp.dot(
+                values_x[block, :, :span], weights, preferred_element_type=jnp.float32
+            )
+
+        def key_step(key_block, _):
+            shift = base - gate_of(key_block)[:, :1]
+            key_at = pl.multiple_of(key_block * seg_len, seg_len)
+            for c in range(seg_len // chunk):
+                cols = slice(c * chunk, (c + 1) * chunk)
+                scores = jnp.dot(
+                    keys_t[pl.ds(key_at, seg_len), :],
+                    queries_x[block, :, cols],
+                    preferred_element_type=jnp.float32,
+                )
+                old = peak[:, cols]
+                top = jnp.maximum(old, jnp.max(scores, axis=0, keepdims=True) + shift)
+                weights = jnp.exp(scores - (top - shift)).astype(jnp.bfloat16)
+                peak[:, cols] = top
+                acc[:, cols] = acc[:, cols] * jnp.exp(old - top) + jnp.dot(
+                    values_x[key_block], weights, preferred_element_type=jnp.float32
+                )
+            return 0
+
+        lax.fori_loop(0, block, key_step, 0)
+        store(block, (acc[:head_dim, :] / acc[head_dim : head_dim + 1, :]).astype(jnp.bfloat16))
+        return 0
+
+    lax.fori_loop(0, seg_count, query_step, 0)
+
+
+def pair_scratch(head_dim, seg_len, seg_count):
+    depth = head_dim + 16
+    return [
+        pltpu.VMEM((seg_len * seg_count, depth), jnp.bfloat16),
+        pltpu.VMEM((seg_count, depth, seg_len), jnp.bfloat16),
+        pltpu.VMEM((seg_count, depth, seg_len), jnp.bfloat16),
+        pltpu.VMEM((depth, seg_len), jnp.float32),
+        pltpu.VMEM((1, seg_len), jnp.float32),
+    ]
+
+
+def attend_by_pair(queries, key_vectors, value_vectors, cumulative_gate):
+    seq_count, feat_width, seg_len = queries.shape
+    heads_here = cumulative_gate.shape[1]
+    head_dim = feat_width // heads_here
+    ep_size = lax.axis_size("ep")
+    share = seq_count * heads_here // ep_size
+
+    def pairs(x):
+        return x.reshape(ep_size, share, 1, head_dim, seg_len)
+
+    sent = jnp.concatenate([pairs(queries), pairs(key_vectors), pairs(value_vectors)], axis=2)
+    got = lax.all_to_all(sent, "ep", split_axis=0, concat_axis=0, tiled=True)
+    gates = lax.dynamic_slice_in_dim(
+        cumulative_gate.reshape(seq_count * heads_here, ep_size, 1, seg_len),
+        lax.axis_index("ep") * share,
+        share,
+        0,
+    )
+
+    def kernel(got_ref, gate_ref, out_ref, *scratch):
+        for p in range(share):
+
+            def store(block, value):
+                out_ref[block, p] = value
+
+            attend_pair(
+                head_dim,
+                seg_len,
+                ep_size,
+                lambda which, block: got_ref[block, p, which],
+                lambda block: gate_ref[p, block],
+                store,
+                *scratch,
+            )
+
+    work = share * head_dim * (seg_len * ep_size) ** 2 * 8
+    out = pl.pallas_call(
+        kernel,
+        out_shape=jax.ShapeDtypeStruct((ep_size, share, head_dim, seg_len), jnp.bfloat16),
+        in_specs=[pl.BlockSpec(memory_space=pltpu.VMEM)] * 2,
+        out_specs=pl.BlockSpec(memory_space=pltpu.VMEM),
+        scratch_shapes=pair_scratch(head_dim, seg_len, ep_size),
+        cost_estimate=pl.CostEstimate(flops=work, bytes_accessed=2 << 20, transcendentals=0),
+        name="attend_by_pair",
+    )(got, gates)
+    back = lax.all_to_all(out, "ep", split_axis=0, concat_axis=0, tiled=True)
+    return back.reshape(seq_count, feat_width, seg_len)
 
 
 def expert_hidden(row_block, route_block, gate_weight, up_weight):
@@ -148,26 +292,19 @@
     places = (
         flat_slot[None, :] == jnp.arange(ep_size * capacity, dtype=jnp.int32)[:, None]
     ).astype(jnp.bfloat16)
+    payload = jnp.concatenate(
+        [normed, routing, jnp.zeros((tok_rows, 128 - group_size), jnp.bfloat16)], axis=1
+    )
     outgoing = (
-        jnp.dot(places, normed, preferred_element_type=jnp.float32)
+        jnp.dot(places, payload, preferred_element_type=jnp.float32)
         .astype(jnp.bfloat16)
-        .reshape(ep_size, capacity, model_dim)
-    )
-    send_route = (
-        jnp.dot(places, routing, preferred_element_type=jnp.float32)
-        .astype(jnp.bfloat16)
-        .reshape(ep_size, capacity, group_size)
-    )
-    arrived, arrived_route = (
-        lax.all_to_all(outgoing, "ep", split_axis=0, concat_axis=0, tiled=True),
-        lax.all_to_all(send_route, "ep", split_axis=0, concat_axis=0, tiled=True),
-    )
-    local_rows = arrived.reshape(ep_size * capacity, model_dim)
-    local_route = arrived_route.reshape(ep_size * capacity, group_size)
-    gathered_rows, gathered_route = (
-        lax.all_gather(local_rows, "tp", axis=0, tiled=True),
-        lax.all_gather(local_route, "tp", axis=0, tiled=True),
-    )
+        .reshape(ep_size, capacity, model_dim + 128)
+    )
+    arrived = lax.all_to_all(outgoing, "ep", split_axis=0, concat_axis=0, tiled=True)
+    local_rows = arrived.reshape(ep_size * capacity, model_dim + 128)
+    gathered = lax.all_gather(local_rows, "tp", axis=0, tiled=True)
+    gathered_rows = gathered[:, :model_dim]
+    gathered_route = gathered[:, model_dim : model_dim + group_size]
     hidden = expert_hidden(gathered_rows, gathered_route, gate_weight, up_weight)
     summed = lax.psum_scatter(
         jnp.einsum("ref,efd->rd", hidden, down_weight, preferred_element_type=jnp.float32).astype(
@@ -200,7 +337,9 @@
     up_weight,
     down_weight,
 ):
-    attention = attend(queries, key_vectors, value_vectors, cumulative_gate)
+    pair_count = queries.shape[0] * cumulative_gate.shape[1]
+    way = attend_by_pair if pair_count % lax.axis_size("ep") == 0 else attend
+    attention = way(queries, key_vectors, value_vectors, cumulative_gate)
     expert_output = mixture(
         expert_input,
         norm_gain,

time: 255 us -> 196 us (0.77)
  matrix products: 54.4 us -> 19.7 us
  Pallas kernels: 0 us -> 27.1 us
  waiting for transfers between devices: 105 us -> 85.6 us
  other arithmetic: 27.9 us -> 9.5 us
  blocking collectives: 34.6 us -> 27.5 us
  local copies, waits for them, and re-layouts: 11.3 us -> 4.27 us
    dot_general x12 -> x1, matrix products: 34.9 us -> 0.33 us  [mixture(): jnp.dot(places, payload, preferred_element_type=jnp.float32)]
    ppermute x4 -> x0, waiting for transfers between devices: 33.6 us -> none  [partner(): lax.ppermute(x, axis, [(i, i ^ 1 << distance) for i in range(lax.axis_siz...]
    pallas_call x0 -> x1, Pallas kernels: none -> 27.1 us  [attend_by_pair(): pl.pallas_call(kernel, out_shape=jax.ShapeDtypeStruct((ep_size, share, he...]
    all_to_all x0 -> x1, waiting for transfers between devices: none -> 19.2 us  [attend_by_pair(): got = lax.all_to_all(sent, 'ep', split_axis=0, concat_axis=0, tiled=True)]
    reduce_sum x5 -> x0, other arithmetic: 17.7 us -> none  [absorb(): total_new = total_old * shrink + jnp.sum(weights, axis=3)]
    all_gather x1 -> x0, blocking collectives: 12.6 us -> none  [mixture(): lax.all_gather(local_route, 'tp', axis=0, tiled=True)]
    all_gather x3 -> x1, waiting for transfers between devices: 69.6 us -> 58.3 us  [mixture(): gathered = lax.all_gather(local_rows, 'tp', axis=0, tiled=True)]
    all_to_all x1, waiting for transfers between devices: 0.01 us -> 8.03 us  [mixture(): lax.all_to_all(summed.reshape(ep_size, capacity, model_dim), 'ep', split_...]
  transfers between devices with their start and end apart: 9 -> 4, of which waited for: 6 -> 3; matrix products, arithmetic and copies ran while one was open for 33% -> 2% of each run, Pallas kernels for 0% -> 14%
where the time goes in v1:
time: 196 us
  waiting for transfers between devices  85.6 us (44%)
  blocking collectives  27.5 us (14%)
  Pallas kernels  27.1 us (14%)
  matrix products  19.7 us (10%)
  between operations  14.1 us (7%)
  other arithmetic  9.5 us (5%)
  starting transfers between devices  7.9 us (4%)
  local copies, waits for them, and re-layouts  4.27 us (2%)
    all_gather x1, waiting for transfers between devices, mixture(): gathered = lax.all_gather(local_rows, 'tp', axis=0, tiled=True)  58.3 us
    pallas_call x1, Pallas kernels, attend_by_pair(): pl.pallas_call(kernel, out_shape=jax.ShapeDtypeStruct((ep_size, share, he...  27.1 us
    all_to_all x1, waiting for transfers between devices, attend_by_pair(): got = lax.all_to_all(sent, 'ep', split_axis=0, concat_axis=0, tiled=True)  19.2 us
    all_to_all x1, blocking collectives, mixture(): lax.all_to_all(outgoing, 'ep', split_axis=0, concat_axis=0, tiled=True)  15.7 us
    all_to_all x1, blocking collectives, attend_by_pair(): back = lax.all_to_all(out, 'ep', split_axis=0, concat_axis=0, tiled=True)  11.8 us
    dot_general x1, matrix products, mixture(): jnp.einsum('ref,efd->rd', hidden, down_weight, preferred_element_type=jnp...  10.5 us
    all_to_all x1, waiting for transfers between devices, mixture(): lax.all_to_all(summed.reshape(ep_size, capacity, model_dim), 'ep', split_...  8.03 us
    dot_general x1, matrix products, expert_hidden(): jnp.einsum('rd,efd->ref', row_block, gate_weight, preferred_element_type=...  7.67 us
  transfers between devices with their start and end apart: 4, of which 3 were waited for; matrix products, arithmetic and copies ran while one was open for 2% of the time, Pallas kernels for 14%

profile of v1, /device:TPU:0, one launch (start us, length us, event | category | flops | bytes accessed | tf_op | source)
XLA Modules:
  0.0 195.6 jit_solution(13640989792445508169)
XLA Ops:
  7.2 0.0 copy-start
  7.2 0.0 all-gather.2.cloned.1.call-start
  7.2 0.8 reduce_max.9
  8.1 0.7 fusion.11
  8.8 0.7 multiply_convert_fusion
  9.5 0.1 copy.23
  9.6 1.2 fusion.5
  10.8 0.7 fusion.8
  11.6 0.2 reduce_window_sum.11
  11.8 0.8 select_reduce_fusion
  12.6 0.7 multiply_add_fusion
  13.3 1.2 fusion.7
  14.5 0.3 concatenate.7
  14.8 0.3 convolution_convert_fusion
  15.1 15.7 %all_to_all.20 = bf16[4,40,2176]{2,1,0:T(8,128)(2,1)} all-to-all(bf16[4,40,2176]{2,1,0:T(8,128)(2,1)S(1)} %bitcast.28), channel_id=1, replica_groups=mesh['ep'=4,'tp'=8] {'ep'}, dimensions={0} | all-to-all | bytes 1392640 | tf_op jit(solution)/shard_map/all_to_all | solution.py:303
  30.8 0.0 all-gather.2.cloned.1.call-update
  30.8 0.0 reduce-scatter.2.cloned.1.call-start
  30.9 58.3 %all-gather.2.cloned.1.call-done = bf16[1280,2176]{1,0:T(8,128)(2,1)} async-done(((bf16[160,2176]{1,0:T(8,128)(2,1)}), bf16[1280,2176]{1,0:T(8,128)(2,1)}) %all-gather.2.cloned.1.call-update) | async-done | bytes 5570576 | tf_op jit(solution)/shard_map/all_gather | solution.py:305
  89.2 1.0 slice.9
  90.2 0.2 copy.25
  90.4 7.7 %fusion.1 = f32[1280,2,256]{2,0,1:T(8,128)} fusion(bf16[2,256,2048]{2,1,0:T(8,128)(2,1)} %param.21, bf16[1280,2176]{1,0:T(8,128)(2,1)} %all-gather.2.cloned.1.call-done), kind=kOutput, calls=%fused_computation.3 | convolution fusion | flops 2684354560 | bytes 9961472 | tf_op jit(solution)/shard_map/rd,efd->ref/dot_general | solution.py:258
  98.0 0.0 copy-done
  98.0 10.5 %bitcast_convert_fusion = bf16[1280,2048]{1,0:T(8,128)(2,1)} fusion(bf16[2,256,2048]{2,1,0:T(8,128)(2,1)S(1)} %copy-done, bf16[2,256,2048]{2,1,0:T(8,128)(2,1)} %param.22, bf16[1280,2176]{1,0:T(8,128)(2,1)} %all-gather.2.cloned.1.call-done, f32[1280,2,256]{2,0,1:T(8,128)} %fusion.1, f32[1280,2]{0,1:T(2,128)S(1)} %convert_element_type.33), kind=kOutput, calls=%fused_computation | convolution fusion | flops 5375918080 | bytes 17311744 | tf_op jit(solution)/shard_map/ref,efd->rd/dot_general | solution.py:310
  108.6 0.0 copy-start.1
  108.6 0.0 copy-start.2
  108.6 0.0 reduce-scatter.2.cloned.1.call-update
  108.6 1.0 copy-done.1
  109.6 0.2 copy-done.2
  109.8 0.0 copy-start.3
  109.8 2.4 %pad_maximum_fusion = bf16[4,1,3,64,1024]{4,3,2,1,0:T(8,128)(2,1)} fusion(bf16[4,1,1,64,1024]{4,3,2,1,0:T(8,128)(2,1)S(1)} %bitcast.32, bf16[4,1,1,64,1024]{4,3,2,1,0:T(8,128)(2,1)S(1)} %bitcast.33, bf16[4,1,1,64,1024]{4,3,2,1,0:T(8,128)(2,1)} %bitcast.34), kind=kLoop, calls=%fused_computation.9 | loop fusion | flops 1572864 | bytes 3145728 | tf_op jit(solution)/shard_map/concatenate | solution.py:218
  112.2 4.3 %all-to-all-start = ((bf16[4,1,3,64,1024]{4,3,2,1,0:T(8,128)(2,1)}), bf16[4,1,3,64,1024]{4,3,2,1,0:T(8,128)(2,1)}, u32[]{:S(2)}, u32[]{:S(2)}) async-start(bf16[4,1,3,64,1024]{4,3,2,1,0:T(8,128)(2,1)} %pad_maximum_fusion), calls=%async_computation | async-start | bytes 3145728 | tf_op jit(solution)/shard_map/all_to_all | solution.py:219
  116.5 0.0 copy-done.3
  116.5 0.1 reshape.49
  116.6 0.6 constant_dynamic-slice_fusion.gate_ref
  117.2 19.2 %all-to-all-done.got_ref = bf16[4,1,3,64,1024]{4,3,2,1,0:T(8,128)(2,1)} async-done(((bf16[4,1,3,64,1024]{4,3,2,1,0:T(8,128)(2,1)}), bf16[4,1,3,64,1024]{4,3,2,1,0:T(8,128)(2,1)}, u32[]{:S(2)}, u32[]{:S(2)}) %all-to-all-start) | async-done | bytes 1572896 | tf_op jit(solution)/shard_map/all_to_all | solution.py:219
  136.5 27.1 %attend_by_pair.1 = bf16[4,1,64,1024]{3,2,1,0:T(8,128)(2,1)} custom-call(bf16[4,1,3,64,1024]{4,3,2,1,0:T(8,128)(2,1)} %all-to-all-done.got_ref, f32[1,4,1,1024]{3,2,1,0:T(1,128)} %constant_dynamic-slice_fusion.gate_ref), custom_call_target="tpu_custom_call" | custom-call | flops 8589934592 | bytes 2097152 | tf_op jit(solution)/shard_map/attend_by_pair/pallas_call | solution.py:244
  163.6 11.8 %all_to_all.21 = bf16[4,1,64,1024]{3,2,1,0:T(8,128)(2,1)S(1)} all-to-all(bf16[4,1,64,1024]{3,2,1,0:T(8,128)(2,1)} %attend_by_pair.1), channel_id=1, replica_groups=mesh['ep'=4,'tp'=8] {'ep'}, dimensions={0} | all-to-all | bytes 1048576 | tf_op jit(solution)/shard_map/all_to_all | solution.py:253
  175.3 0.0 reduce-scatter.2.cloned.1.call-done
  175.3 3.5 %all-to-all-start.3 = ((bf16[4,40,2048]{2,1,0:T(8,128)(2,1)}), bf16[4,40,2048]{2,1,0:T(8,128)(2,1)S(1)}, u32[]{:S(2)}, u32[]{:S(2)}) async-start(bf16[4,40,2048]{2,1,0:T(8,128)(2,1)} %bitcast.31), calls=%async_computation.4 | async-start | bytes 1310720 | tf_op jit(solution)/shard_map/all_to_all | solution.py:317
  178.8 8.0 %all-to-all-done.3 = bf16[4,40,2048]{2,1,0:T(8,128)(2,1)S(1)} async-done(((bf16[4,40,2048]{2,1,0:T(8,128)(2,1)}), bf16[4,40,2048]{2,1,0:T(8,128)(2,1)S(1)}, u32[]{:S(2)}, u32[]{:S(2)}) %all-to-all-start.3) | async-done | bytes 655392 | tf_op jit(solution)/shard_map/all_to_all | solution.py:317
  186.9 1.1 convolution_convert_fusion.1
  188.0 0.8 copy.27
  (3 shorter events, 0.0 us)
Async XLA Ops:
  7.2 90.9 %copy-start = (bf16[2,256,2048]{2,1,0:T(8,128)(2,1)S(1)}, bf16[2,256,2048]{2,1,0:T(8,128)(2,1)}, u32[]{:S(2)}) copy-start(bf16[2,256,2048]{2,1,0:T(8,128)(2,1)} %param.23) | copy-start | bytes 6291460
  7.2 82.0 %all-gather.2.cloned.1.call-start = ((), (), s32[]{:S(2)}) async-start(), calls=%async_computation.5 | async-start | bytes 6266880 | tf_op jit(solution)/shard_map/all_gather | solution.py:305
  30.8 144.5 %reduce-scatter.2.cloned.1.call-start = ((), (), s32[]{:S(2)}) async-start(), calls=%async_computation.6 | async-start | bytes 5898240 | tf_op jit(solution)/shard_map/reduce_scatter | solution.py:309
  108.6 1.0 copy-start.1
  108.6 1.2 copy-start.2
  109.8 6.7 %copy-start.3 = (f32[2,2,4096]{2,1,0:T(2,128)S(1)}, f32[2,2,4096]{2,1,0:T(2,128)}, u32[]{:S(2)}) copy-start(f32[2,2,4096]{2,1,0:T(2,128)} %param.15) | copy-start | bytes 196612
  112.2 24.3 %all-to-all-start = ((bf16[4,1,3,64,1024]{4,3,2,1,0:T(8,128)(2,1)}), bf16[4,1,3,64,1024]{4,3,2,1,0:T(8,128)(2,1)}, u32[]{:S(2)}, u32[]{:S(2)}) async-start(bf16[4,1,3,64,1024]{4,3,2,1,0:T(8,128)(2,1)} %pad_maximum_fusion), calls=%async_computation | async-start | bytes 3145728 | tf_op jit(solution)/shard_map/all_to_all | solution.py:219
  175.3 11.5 %all-to-all-start.3 = ((bf16[4,40,2048]{2,1,0:T(8,128)(2,1)}), bf16[4,40,2048]{2,1,0:T(8,128)(2,1)S(1)}, u32[]{:S(2)}, u32[]{:S(2)}) async-start(bf16[4,40,2048]{2,1,0:T(8,128)(2,1)} %bitcast.31), calls=%async_computation.4 | async-start | bytes 1310720 | tf_op jit(solution)/shard_map/all_to_all | solution.py:317
Sparse Core Ops, SparseCore 0:
  31.0 58.1 all-gather.1
  108.7 58.5 reduce-scatter.1

commit v2 on v1

--- a/solution.py
+++ b/solution.py
@@ -240,7 +240,7 @@
                 *scratch,
             )
 
-    work = share * head_dim * (seg_len * ep_size) ** 2 * 8
+    work = share * head_dim * (seg_len * ep_size) ** 2 * 24
     out = pl.pallas_call(
         kernel,
         out_shape=jax.ShapeDtypeStruct((ep_size, share, head_dim, seg_len), jnp.bfloat16),
@@ -254,12 +254,184 @@
     return back.reshape(seq_count, feat_width, seg_len)
 
 
-def expert_hidden(row_block, route_block, gate_weight, up_weight):
-    gate_act = jnp.einsum("rd,efd->ref", row_block, gate_weight, preferred_element_type=jnp.float32)
-    up_act = jnp.einsum("rd,efd->ref", row_block, up_weight, preferred_element_type=jnp.float32)
-    return (jax.nn.silu(gate_act) * up_act * route_block.astype(jnp.float32)[:, :, None]).astype(
-        jnp.bfloat16
-    )
+def experts_on_line(gathered, gate_weight, up_weight, down_weight):
+    n_tp, rows, width = gathered.shape
+    group_size, hidden_width, model_dim = gate_weight.shape
+    chips = n_tp // 2
+    last = chips - 1
+
+    def kernel(
+        rows_ref, gate_ref, up_ref, down_ref, out_ref,
+        part, sums, pair_out, pair_in, line_out, line_in,
+        pair_ss, pair_rs, line_ss, line_rs,
+    ):
+        tp = lax.axis_index("tp")
+        z = tp // 2
+        core = tp % 2
+        sibling = z * 2 + 1 - core
+        barrier = pltpu.get_barrier_semaphore()
+
+        def greet(other):
+            pl.semaphore_signal(
+                barrier, inc=1, device_id={"tp": other}, device_id_type=pl.DeviceIdType.MESH
+            )
+
+        greet(sibling)
+
+        @pl.when(z > 0)
+        def _():
+            greet(tp - 2)
+
+        @pl.when(z < last)
+        def _():
+            greet(tp + 2)
+
+        inside = (z > 0) & (z < last)
+
+        @pl.when(inside)
+        def _():
+            pl.semaphore_wait(barrier, 3)
+
+        @pl.when(jnp.logical_not(inside))
+        def _():
+            pl.semaphore_wait(barrier, 2 if last > 0 else 1)
+
+        def pair_copy(t):
+            return pltpu.make_async_remote_copy(
+                pair_out.at[t], pair_in.at[t], pair_ss.at[t], pair_rs.at[t],
+                device_id={"tp": sibling}, device_id_type=pl.DeviceIdType.MESH,
+            )
+
+        def line_copy(t, slot, other):
+            return pltpu.make_async_remote_copy(
+                line_out.at[t], line_in.at[slot], line_ss.at[t], line_rs.at[slot],
+                device_id={"tp": other}, device_id_type=pl.DeviceIdType.MESH,
+            )
+
+        def send_right(t):
+            line_copy(t, t, tp + 2).start()
+
+        def send_left(t):
+            @pl.when(t == z - 1)
+            def _():
+                line_copy(t, chips, tp - 2).start()
+
+            @pl.when(t < z - 1)
+            def _():
+                line_copy(t, t, tp - 2).start()
+
+        upper = (2 * z) // chips
+
+        def compute(i, _):
+            t = (1 - upper) * (last - i) + upper * i
+            block = rows_ref[pl.ds(t * 2, 2)].reshape(2 * rows, width)
+            tokens = block[:, :model_dim]
+            route = block[:, model_dim:].astype(jnp.float32)
+            for e in range(group_size):
+                nt = (((1,), (1,)), ((), ()))
+                gate_act = lax.dot_general(
+                    tokens, gate_ref[e], nt, preferred_element_type=jnp.float32
+                )
+                up_act = lax.dot_general(tokens, up_ref[e], nt, preferred_element_type=jnp.float32)
+                hidden = gate_act / (1.0 + jnp.exp(-gate_act)) * up_act * route[:, e : e + 1]
+                term = jnp.dot(
+                    hidden.astype(jnp.bfloat16), down_ref[e], preferred_element_type=jnp.float32
+                ).reshape(2, rows, model_dim)
+                if e == 0:
+                    part[...] = term
+                else:
+                    part[...] += term
+            pair_out[t] = part[1 - core].astype(jnp.bfloat16)
+            copy = pair_copy(t)
+            copy.start()
+            copy.wait_recv()
+            sums[t] = part[core] + pair_in[t].astype(jnp.float32)
+
+            @pl.when((z == 0) & (t > 0))
+            def _():
+                line_out[t] = sums[t].astype(jnp.bfloat16)
+                send_right(t)
+
+            @pl.when((z == last) & (t < last))
+            def _():
+                line_out[t] = sums[t].astype(jnp.bfloat16)
+                send_left(t)
+
+            return 0
+
+        lax.fori_loop(0, chips, compute, 0)
+
+        def pass_on(k, _):
+            right_t = last - (k - z)
+            left_t = k - (last - z)
+
+            @pl.when((z > 0) & (k >= z) & (right_t > z))
+            def _():
+                line_copy(right_t, right_t, tp).wait_recv()
+                line_out[right_t] = (
+                    sums[right_t] + line_in[right_t].astype(jnp.float32)
+                ).astype(jnp.bfloat16)
+                send_right(right_t)
+
+            @pl.when((z < last) & (left_t >= 0) & (left_t < z))
+            def _():
+                line_copy(left_t, left_t, tp).wait_recv()
+                line_out[left_t] = (
+                    sums[left_t] + line_in[left_t].astype(jnp.float32)
+                ).astype(jnp.bfloat16)
+                send_left(left_t)
+
+            return 0
+
+        lax.fori_loop(1, chips, pass_on, 0)
+
+        @pl.when(z > 0)
+        def _():
+            line_copy(z, z, tp).wait_recv()
+            sums[z] = sums[z] + line_in[z].astype(jnp.float32)
+
+        @pl.when(z < last)
+        def _():
+            line_copy(z, chips, tp).wait_recv()
+            sums[z] = sums[z] + line_in[chips].astype(jnp.float32)
+
+        out_ref[...] = sums[z].astype(jnp.bfloat16)
+
+        def drain(t, _):
+            pair_copy(t).wait_send()
+
+            @pl.when(t != z)
+            def _():
+                line_copy(t, t, tp).wait_send()
+
+            return 0
+
+        lax.fori_loop(0, chips, drain, 0)
+
+    flops = 6 * n_tp * rows * group_size * hidden_width * model_dim
+    return pl.pallas_call(
+        kernel,
+        out_shape=jax.ShapeDtypeStruct((rows, model_dim), jnp.bfloat16),
+        in_specs=[pl.BlockSpec(memory_space=pltpu.VMEM)] * 4,
+        out_specs=pl.BlockSpec(memory_space=pltpu.VMEM),
+        scratch_shapes=[
+            pltpu.VMEM((2, rows, model_dim), jnp.float32),
+            pltpu.VMEM((chips, rows, model_dim), jnp.float32),
+            pltpu.VMEM((chips, rows, model_dim), jnp.bfloat16),
+            pltpu.VMEM((chips, rows, model_dim), jnp.bfloat16),
+            pltpu.VMEM((chips, rows, model_dim), jnp.bfloat16),
+            pltpu.VMEM((chips + 1, rows, model_dim), jnp.bfloat16),
+            pltpu.SemaphoreType.DMA((chips,)),
+            pltpu.SemaphoreType.DMA((chips,)),
+            pltpu.SemaphoreType.DMA((chips,)),
+            pltpu.SemaphoreType.DMA((chips + 1,)),
+        ],
+        compiler_params=pltpu.CompilerParams(
+            collective_id=0, has_side_effects=True, vmem_limit_bytes=63 << 20
+        ),
+        cost_estimate=pl.CostEstimate(flops=4 * flops, bytes_accessed=12 << 20, transcendentals=0),
+        name="experts_on_line",
+    )(gathered, gate_weight, up_weight, down_weight)
 
 
 def mixture(
@@ -302,18 +474,8 @@
     )
     arrived = lax.all_to_all(outgoing, "ep", split_axis=0, concat_axis=0, tiled=True)
     local_rows = arrived.reshape(ep_size * capacity, model_dim + 128)
-    gathered = lax.all_gather(local_rows, "tp", axis=0, tiled=True)
-    gathered_rows = gathered[:, :model_dim]
-    gathered_route = gathered[:, model_dim : model_dim + group_size]
-    hidden = expert_hidden(gathered_rows, gathered_route, gate_weight, up_weight)
-    summed = lax.psum_scatter(
-        jnp.einsum("ref,efd->rd", hidden, down_weight, preferred_element_type=jnp.float32).astype(
-            jnp.bfloat16
-        ),
-        "tp",
-        scatter_dimension=0,
-        tiled=True,
-    )
+    gathered = lax.all_gather(local_rows, "tp", axis=0)
+    summed = experts_on_line(gathered, gate_weight, up_weight, down_weight)
     returned = lax.all_to_all(
         summed.reshape(ep_size, capacity, model_dim), "ep", split_axis=0, concat_axis=0, tiled=True
     )

time: 196 us -> 169 us (0.86)
  Pallas kernels: 27.1 us -> 85.7 us
  waiting for transfers between devices: 85.6 us -> 29.3 us
  matrix products: 19.7 us -> 1.47 us
  blocking collectives: 27.5 us -> 15.8 us
  starting transfers between devices: 7.9 us -> 10.9 us
    pallas_call x0 -> x1, Pallas kernels: none -> 58.6 us  [experts_on_line(): pl.pallas_call(kernel, out_shape=jax.ShapeDtypeStruct((rows, model_dim),...]
    all_gather x1, waiting for transfers between devices: 58.3 us -> 3.26 us  [mixture(): gathered = lax.all_gather(local_rows, 'tp', axis=0)]
    dot_general x2 -> x0, matrix products: 18.2 us -> none  [the longest x1 10.5 us: mixture(): jnp.einsum('ref,efd->rd', hidden, down_weight, preferred_element_type=jnp...]
    all_to_all x1 -> x0, blocking collectives: 11.8 us -> none  [attend_by_pair(): back = lax.all_to_all(out, 'ep', split_axis=0, concat_axis=0, tiled=True)]
    all_to_all x0 -> x1, starting transfers between devices: none -> 3.47 us  [attend_by_pair(): back = lax.all_to_all(out, 'ep', split_axis=0, concat_axis=0, tiled=True)]
  transfers between devices with their start and end apart: 4 -> 4, of which waited for: 3 -> 3; matrix products, arithmetic and copies ran while one was open for 2% -> 1% of each run, Pallas kernels for 14% -> 51%
where the time goes in v2:
time: 169 us
  Pallas kernels  85.7 us (51%)
  waiting for transfers between devices  29.3 us (17%)
  blocking collectives  15.8 us (9%)
  between operations  14.2 us (8%)
  starting transfers between devices  10.9 us (6%)
  other arithmetic  8.31 us (5%)
  local copies, waits for them, and re-layouts  3.11 us (2%)
    pallas_call x1, Pallas kernels, experts_on_line(): pl.pallas_call(kernel, out_shape=jax.ShapeDtypeStruct((rows, model_dim),...  58.6 us
    pallas_call x1, Pallas kernels, attend_by_pair(): pl.pallas_call(kernel, out_shape=jax.ShapeDtypeStruct((ep_size, share, he...  27.1 us
    all_to_all x1, waiting for transfers between devices, attend_by_pair(): got = lax.all_to_all(sent, 'ep', split_axis=0, concat_axis=0, tiled=True)  17.5 us
    all_to_all x1, blocking collectives, mixture(): lax.all_to_all(outgoing, 'ep', split_axis=0, concat_axis=0, tiled=True)  15.8 us
    all_to_all x1, waiting for transfers between devices, mixture(): lax.all_to_all(summed.reshape(ep_size, capacity, model_dim), 'ep', split_...  8.5 us
    all_to_all x1, starting transfers between devices, attend_by_pair(): got = lax.all_to_all(sent, 'ep', split_axis=0, concat_axis=0, tiled=True)  3.69 us
    all_to_all x1, starting transfers between devices, mixture(): lax.all_to_all(summed.reshape(ep_size, capacity, model_dim), 'ep', split_...  3.66 us
    all_to_all x1, starting transfers between devices, attend_by_pair(): back = lax.all_to_all(out, 'ep', split_axis=0, concat_axis=0, tiled=True)  3.47 us
  transfers between devices with their start and end apart: 4, of which 3 were waited for; matrix products, arithmetic and copies ran while one was open for 1% of the time, Pallas kernels for 51%

profile of v2, /device:TPU:0, one launch (start us, length us, event | category | flops | bytes accessed | tf_op | source)
XLA Modules:
  0.0 168.7 jit_solution(3966684483069926080)
XLA Ops:
  7.2 0.0 all-gather.2.cloned.1.call-start
  7.2 0.7 reduce_max.9
  7.9 0.7 fusion.6
  8.6 1.2 fusion
  9.8 0.7 multiply_convert_fusion
  10.5 0.1 copy.15
  10.7 0.7 fusion.3
  11.4 0.2 reduce_window_sum.11
  11.6 0.8 select_reduce_fusion
  12.4 0.7 multiply_add_fusion
  13.1 1.2 fusion.2
  14.3 0.3 concatenate.7
  14.6 0.0 copy-start.1
  14.6 0.0 copy-start.2
  14.6 0.0 copy-start.3
  14.7 0.3 convolution_convert_fusion
  15.0 15.8 %all_to_all.20 = bf16[4,40,2176]{2,1,0:T(8,128)(2,1)} all-to-all(bf16[4,40,2176]{2,1,0:T(8,128)(2,1)S(1)} %bitcast.11), channel_id=1, replica_groups=mesh['ep'=4,'tp'=8] {'ep'}, dimensions={0} | all-to-all | bytes 1392640 | tf_op jit(solution)/shard_map/all_to_all | solution.py:475
  30.8 0.0 all-gather.2.cloned.1.call-update
  30.9 0.0 copy-done.1
  30.9 0.0 copy-done.2
  30.9 0.0 copy-done.3
  30.9 1.3 pad_maximum_fusion
  32.2 0.0 copy-start.4
  32.2 3.7 %all-to-all-start = ((bf16[4,1,3,64,1024]{4,3,2,1,0:T(8,128)(2,1)}), bf16[4,1,3,64,1024]{4,3,2,1,0:T(8,128)(2,1)S(1)}, u32[]{:S(2)}, u32[]{:S(2)}) async-start(bf16[4,1,3,64,1024]{4,3,2,1,0:T(8,128)(2,1)} %pad_maximum_fusion), calls=%async_computation | async-start | bytes 3145728 | tf_op jit(solution)/shard_map/all_to_all | solution.py:219
  35.9 0.0 copy-done.4
  35.9 0.1 reshape.45
  36.1 0.6 constant_dynamic-slice_fusion.gate_ref
  36.7 17.5 %all-to-all-done.got_ref = bf16[4,1,3,64,1024]{4,3,2,1,0:T(8,128)(2,1)S(1)} async-done(((bf16[4,1,3,64,1024]{4,3,2,1,0:T(8,128)(2,1)}), bf16[4,1,3,64,1024]{4,3,2,1,0:T(8,128)(2,1)S(1)}, u32[]{:S(2)}, u32[]{:S(2)}) %all-to-all-start) | async-done | bytes 1572896 | tf_op jit(solution)/shard_map/all_to_all | solution.py:219
  54.2 0.0 copy-start
  54.2 1.2 copy-done
  55.4 27.1 %attend_by_pair.1 = bf16[4,1,64,1024]{3,2,1,0:T(8,128)(2,1)} custom-call(bf16[4,1,3,64,1024]{4,3,2,1,0:T(8,128)(2,1)} %copy-done, f32[1,4,1,1024]{3,2,1,0:T(1,128)} %constant_dynamic-slice_fusion.gate_ref), custom_call_target="tpu_custom_call" | custom-call | flops 25769803776 | bytes 2097152 | tf_op jit(solution)/shard_map/attend_by_pair/pallas_call | solution.py:244
  82.5 3.5 %all-to-all-start.1 = ((bf16[4,1,64,1024]{3,2,1,0:T(8,128)(2,1)}), bf16[4,1,64,1024]{3,2,1,0:T(8,128)(2,1)S(1)}, u32[]{:S(2)}, u32[]{:S(2)}) async-start(bf16[4,1,64,1024]{3,2,1,0:T(8,128)(2,1)} %attend_by_pair.1), calls=%async_computation.1 | async-start | bytes 1048576 | tf_op jit(solution)/shard_map/all_to_all | solution.py:253
  85.9 3.3 %all-gather.2.cloned.1.call-done.rows_ref = bf16[8,160,2176]{2,1,0:T(8,128)(2,1)} async-done(((bf16[1,160,2176]{2,1,0:T(8,128)(2,1)}), bf16[8,160,2176]{2,1,0:T(8,128)(2,1)}) %all-gather.2.cloned.1.call-update) | async-done | bytes 5570576 | tf_op jit(solution)/shard_map/all_gather | solution.py:477
  89.2 58.6 %experts_on_line.1 = bf16[160,2048]{1,0:T(8,128)(2,1)} custom-call(bf16[8,160,2176]{2,1,0:T(8,128)(2,1)} %all-gather.2.cloned.1.call-done.rows_ref, bf16[2,256,2048]{2,1,0:T(8,128)(2,1)} %gate_ref.1, bf16[2,256,2048]{2,1,0:T(8,128)(2,1)} %up_ref.1, bf16[2,256,2048]{2,1,0:T(8,128)(2,1)} %down_ref.1), custom_call_target="tpu_custom_call" | custom-call | flops 32212254720 | bytes 12582912 | tf_op jit(solution)/shard_map/experts_on_line/pallas_call | solution.py:412
  147.8 0.0 all-to-all-done.1
  147.8 3.7 %all-to-all-start.3 = ((bf16[4,40,2048]{2,1,0:T(8,128)(2,1)}), bf16[4,40,2048]{2,1,0:T(8,128)(2,1)S(1)}, u32[]{:S(2)}, u32[]{:S(2)}) async-start(bf16[4,40,2048]{2,1,0:T(8,128)(2,1)} %bitcast.14), calls=%async_computation.3 | async-start | bytes 1310720 | tf_op jit(solution)/shard_map/all_to_all | solution.py:479
  151.5 8.5 %all-to-all-done.3 = bf16[4,40,2048]{2,1,0:T(8,128)(2,1)S(1)} async-done(((bf16[4,40,2048]{2,1,0:T(8,128)(2,1)}), bf16[4,40,2048]{2,1,0:T(8,128)(2,1)S(1)}, u32[]{:S(2)}, u32[]{:S(2)}) %all-to-all-start.3) | async-done | bytes 655392 | tf_op jit(solution)/shard_map/all_to_all | solution.py:479
  160.0 1.1 convolution_convert_fusion.1
  161.1 0.8 copy.17
  (2 shorter events, 0.0 us)
Async XLA Ops:
  7.2 82.0 %all-gather.2.cloned.1.call-start = ((), (), s32[]{:S(2)}) async-start(), calls=%async_computation.4 | async-start | bytes 6266880 | tf_op jit(solution)/shard_map/all_gather | solution.py:477
  14.6 16.2 %copy-start.1 = (bf16[2,128,1024]{2,1,0:T(8,128)(2,1)S(1)}, bf16[2,128,1024]{2,1,0:T(8,128)(2,1)}, u32[]{:S(2)}) copy-start(bf16[2,128,1024]{2,1,0:T(8,128)(2,1)} %param.14) | copy-start | bytes 1572868
  14.6 16.2 %copy-start.2 = (bf16[2,128,1024]{2,1,0:T(8,128)(2,1)S(1)}, bf16[2,128,1024]{2,1,0:T(8,128)(2,1)}, u32[]{:S(2)}) copy-start(bf16[2,128,1024]{2,1,0:T(8,128)(2,1)} %param.13) | copy-start | bytes 1572868
  14.6 16.2 %copy-start.3 = (bf16[2,128,1024]{2,1,0:T(8,128)(2,1)S(1)}, bf16[2,128,1024]{2,1,0:T(8,128)(2,1)}, u32[]{:S(2)}) copy-start(bf16[2,128,1024]{2,1,0:T(8,128)(2,1)} %param.12) | copy-start | bytes 1572868
  32.2 3.7 %copy-start.4 = (f32[2,2,4096]{2,1,0:T(2,128)S(1)}, f32[2,2,4096]{2,1,0:T(2,128)}, u32[]{:S(2)}) copy-start(f32[2,2,4096]{2,1,0:T(2,128)} %param.15) | copy-start | bytes 196612
  32.2 22.0 %all-to-all-start = ((bf16[4,1,3,64,1024]{4,3,2,1,0:T(8,128)(2,1)}), bf16[4,1,3,64,1024]{4,3,2,1,0:T(8,128)(2,1)S(1)}, u32[]{:S(2)}, u32[]{:S(2)}) async-start(bf16[4,1,3,64,1024]{4,3,2,1,0:T(8,128)(2,1)} %pad_maximum_fusion), calls=%async_computation | async-start | bytes 3145728 | tf_op jit(solution)/shard_map/all_to_all | solution.py:219
  54.2 1.2 copy-start
  82.5 65.3 %all-to-all-start.1 = ((bf16[4,1,64,1024]{3,2,1,0:T(8,128)(2,1)}), bf16[4,1,64,1024]{3,2,1,0:T(8,128)(2,1)S(1)}, u32[]{:S(2)}, u32[]{:S(2)}) async-start(bf16[4,1,64,1024]{3,2,1,0:T(8,128)(2,1)} %attend_by_pair.1), calls=%async_computation.1 | async-start | bytes 1048576 | tf_op jit(solution)/shard_map/all_to_all | solution.py:253
  147.8 12.2 %all-to-all-start.3 = ((bf16[4,40,2048]{2,1,0:T(8,128)(2,1)}), bf16[4,40,2048]{2,1,0:T(8,128)(2,1)S(1)}, u32[]{:S(2)}, u32[]{:S(2)}) async-start(bf16[4,40,2048]{2,1,0:T(8,128)(2,1)} %bitcast.14), calls=%async_computation.3 | async-start | bytes 1310720 | tf_op jit(solution)/shard_map/all_to_all | solution.py:479
Sparse Core Ops, SparseCore 0:
  31.0 58.1 all-gather.1
